TPU v7x, 32 devices: a whole 2x2x4 slice. The times are simulated.
32 devices in a mesh: ra: 4 (over z), cb: 4 (over y, x), dp: 2 (over core).
Axes of the slice: x: 2, y: 2, z: 4, core: 2. Of those that a mesh axis runs over, the one named last changes fastest.
Arguments:
- tokens: bfloat16 [384, 4096], P('dp', 'ra'), may hold values from -13 to 13, as said below
- gate_first: bfloat16 [4096, 11264], P('ra', 'cb'), may hold values from -0.125 to 0.125
- up_first: bfloat16 [4096, 11264], P('ra', 'cb'), may hold values from -0.125 to 0.125
- down_first: bfloat16 [11264, 4096], P('cb', 'ra'), may hold values from -0.0546875 to 0.0546875
- gain_first: float32 [4096], P('ra'), may hold values from 0.1 to 1.9
- shift_first: float32 [4096], P('ra'), may hold values from -3 to 3
- gate_second: bfloat16 [4096, 11264], P('ra', 'cb'), may hold values from -0.125 to 0.125
- up_second: bfloat16 [4096, 11264], P('ra', 'cb'), may hold values from -0.125 to 0.125
- down_second: bfloat16 [11264, 4096], P('cb', 'ra'), may hold values from -0.0546875 to 0.0546875
- gain_second: float32 [4096], P('ra'), may hold values from 0.1 to 1.9
- shift_second: float32 [4096], P('ra'), may hold values from -3 to 3
Outputs:
- result: bfloat16 [384, 4096], P('dp', 'ra')
Inputs may be any that keep to these rules, and one draw needn't show every extreme that they name: `tokens`: input activations whose blocks of 64 consecutive features have their own scale and offset.
All inputs are finite; a program needn't handle non-finite values.
Results may differ from a plain program's by a relative error of at most 0.0066.
Values may be sent and summed in bfloat16 or wider, within the bound.
A program may use at most 128 MiB of HBM per device.

v0:
```python
import jax
import jax.numpy as jnp
from jax import lax
from jax.sharding import PartitionSpec as P

D = 4096


def normalize(mixed, gain, bias):
    total, squares = lax.psum(
        (jnp.sum(mixed, axis=-1, keepdims=True), jnp.sum(mixed * mixed, axis=-1, keepdims=True)),
        "ra",
    )
    mean = total / D
    variance = squares / D - mean * mean
    centered = mixed - mean
    return centered * lax.rsqrt(variance + 1e-05) * gain + bias


def half_step(values, gate, up, down, gain, bias):
    gate_part = jnp.dot(values, gate, preferred_element_type=jnp.float32)
    up_part = jnp.dot(values, up, preferred_element_type=jnp.float32)
    gate_pre, up_pre = (
        lax.psum_scatter(gate_part, "ra", scatter_dimension=0, tiled=True),
        lax.psum_scatter(up_part, "ra", scatter_dimension=0, tiled=True),
    )
    hidden = (jax.nn.silu(gate_pre) * up_pre).astype(jnp.bfloat16)
    partial_value = jnp.dot(
        lax.all_gather(hidden, "ra", axis=0, tiled=True), down, preferred_element_type=jnp.float32
    )
    branch = lax.psum(partial_value, "cb")
    mixed = 0.25 * values.astype(jnp.float32) + 0.5 * branch
    return normalize(mixed, gain, bias).astype(jnp.bfloat16)


def on_device(
    tokens,
    gate_first,
    up_first,
    down_first,
    gain_first,
    shift_first,
    gate_second,
    up_second,
    down_second,
    gain_second,
    shift_second,
):
    middle = half_step(tokens, gate_first, up_first, down_first, gain_first, shift_first)
    return half_step(middle, gate_second, up_second, down_second, gain_second, shift_second)


def solution(mesh):
    in_specs = (
        P("dp", "ra"),
        P("ra", "cb"),
        P("ra", "cb"),
        P("cb", "ra"),
        P("ra"),
        P("ra"),
        P("ra", "cb"),
        P("ra", "cb"),
        P("cb", "ra"),
        P("ra"),
        P("ra"),
    )
    out_specs = P("dp", "ra")
    return jax.shard_map(
        on_device, mesh=mesh, in_specs=in_specs, out_specs=out_specs, check_vma=False
    )
```

profile of v0, /device:TPU:0, one launch (start us, length us, event | category | flops | bytes accessed | tf_op | source)
XLA Modules:
  0.0 402.7 jit_solution(13173564124745318421)
XLA Ops:
  6.5 5.5 %fusion.2 = f32[192,2816]{1,0:T(8,128)} fusion(bf16[192,1024]{1,0:T(8,128)(2,1)} %param.11, bf16[1024,2816]{1,0:T(8,128)(2,1)} %param.12), kind=kOutput, calls=%fused_computation.14 | convolution fusion | flops 1107296256 | bytes 8323072 | tf_op jit(solution)/shard_map/dot_general | solution.py:21
  12.0 0.0 reduce-scatter.7.cloned.1.call-start
  12.1 5.3 %fusion.3 = f32[192,2816]{1,0:T(8,128)} fusion(bf16[192,1024]{1,0:T(8,128)(2,1)S(1)} %copy-done, bf16[1024,2816]{1,0:T(8,128)(2,1)} %param.13), kind=kOutput, calls=%fused_computation.15 | convolution fusion | flops 1107296256 | bytes 8323072 | tf_op jit(solution)/shard_map/dot_general | solution.py:22
  17.4 0.0 all-gather.3.cloned.1.call-start
  17.4 42.1 %reduce-scatter.5.cloned.1.call-done = f32[48,2816]{1,0:T(8,128)} async-done(((f32[192,2816]{1,0:T(8,128)}), f32[48,2816]{1,0:T(8,128)}) %reduce-scatter.5.cloned.1.call-update) | async-done | bytes 540688 | tf_op jit(solution)/shard_map/reduce_scatter | solution.py:24
  59.5 46.2 %reduce-scatter.7.cloned.1.call-done = f32[48,2816]{1,0:T(8,128)} async-done(((f32[192,2816]{1,0:T(8,128)}), f32[48,2816]{1,0:T(8,128)}) %reduce-scatter.7.cloned.1.call-update) | async-done | bytes 540688 | tf_op jit(solution)/shard_map/reduce_scatter | solution.py:25
  105.8 2.1 multiply_convert_fusion.1
  107.9 27.9 %all-gather.3.cloned.1.call-done = bf16[192,2816]{1,0:T(8,128)(2,1)} async-done(((bf16[48,2816]{1,0:T(8,128)(2,1)}), bf16[192,2816]{1,0:T(8,128)(2,1)}) %all-gather.3.cloned.1.call-update) | async-done | bytes 1081360 | tf_op jit(solution)/shard_map/all_gather | solution.py:29
  135.8 5.2 %fusion.4 = f32[192,1024]{1,0:T(8,128)} fusion(bf16[192,2816]{1,0:T(8,128)(2,1)} %all-gather.3.cloned.1.call-done, bf16[2816,1024]{1,0:T(8,128)(2,1)} %param.14), kind=kOutput, calls=%fused_computation.16 | convolution fusion | flops 1107296256 | bytes 7634944 | tf_op jit(solution)/shard_map/dot_general | solution.py:28
  141.1 48.1 %all-reduce.5.cloned.1.call-done = f32[192,1024]{1,0:T(8,128)} async-done(((f32[192,1024]{1,0:T(8,128)}), f32[192,1024]{1,0:T(8,128)}) %all-reduce.5.cloned.1.call-update) | async-done | bytes 786448 | tf_op jit(solution)/shard_map/psum | solution.py:31
  189.2 1.4 fusion
  190.6 11.7 %all-reduce.1 = (f32[192,1]{0,1:T(1,128)S(1)}, f32[192,1]{0,1:T(1,128)S(1)}) all-reduce(f32[192,1]{0,1:T(1,128)S(1)} %bitcast.21, f32[192,1]{0,1:T(1,128)S(1)} %bitcast.20), channel_id=1, replica_groups=mesh['ra'=4,'cb'=4,'dp'=2] {'ra'}, use_global_device_ids=true, to_apply=%region_6.7 | all-reduce | flops 384 | bytes 3072 | tf_op jit(solution)/shard_map/psum | solution.py:10
  202.3 1.4 add_convert_fusion.1
  203.7 5.3 %fusion.6 = f32[192,2816]{1,0:T(8,128)} fusion(bf16[192,1024]{1,0:T(8,128)(2,1)S(1)} %add_convert_fusion.1, bf16[1024,2816]{1,0:T(8,128)(2,1)} %param.18), kind=kOutput, calls=%fused_computation.18 | convolution fusion | flops 1107296256 | bytes 8323072 | tf_op jit(solution)/shard_map/dot_general | solution.py:22
  209.1 5.3 %fusion.5 = f32[192,2816]{1,0:T(8,128)} fusion(bf16[192,1024]{1,0:T(8,128)(2,1)S(1)} %add_convert_fusion.1, bf16[1024,2816]{1,0:T(8,128)(2,1)} %param.17), kind=kOutput, calls=%fused_computation.17 | convolution fusion | flops 1107296256 | bytes 8323072 | tf_op jit(solution)/shard_map/dot_general | solution.py:21
  214.4 36.6 %reduce-scatter.11.cloned.1.call-done = f32[48,2816]{1,0:T(8,128)} async-done(((f32[192,2816]{1,0:T(8,128)}), f32[48,2816]{1,0:T(8,128)}) %reduce-scatter.11.cloned.1.call-update) | async-done | bytes 540688 | tf_op jit(solution)/shard_map/reduce_scatter | solution.py:25
  251.1 46.1 %reduce-scatter.9.cloned.1.call-done = f32[48,2816]{1,0:T(8,128)} async-done(((f32[192,2816]{1,0:T(8,128)}), f32[48,2816]{1,0:T(8,128)}) %reduce-scatter.9.cloned.1.call-update) | async-done | bytes 540688 | tf_op jit(solution)/shard_map/reduce_scatter | solution.py:24
  297.1 2.1 multiply_convert_fusion
  299.3 27.8 %all-gather.5.cloned.1.call-done = bf16[192,2816]{1,0:T(8,128)(2,1)} async-done(((bf16[48,2816]{1,0:T(8,128)(2,1)}), bf16[192,2816]{1,0:T(8,128)(2,1)}) %all-gather.5.cloned.1.call-update) | async-done | bytes 1081360 | tf_op jit(solution)/shard_map/all_gather | solution.py:29
  327.2 5.2 %fusion.7 = f32[192,1024]{1,0:T(8,128)} fusion(bf16[192,2816]{1,0:T(8,128)(2,1)} %all-gather.5.cloned.1.call-done, bf16[2816,1024]{1,0:T(8,128)(2,1)} %param.19), kind=kOutput, calls=%fused_computation.19 | convolution fusion | flops 1107296256 | bytes 7634944 | tf_op jit(solution)/shard_map/dot_general | solution.py:28
  332.4 48.2 %all-reduce.7.cloned.1.call-done = f32[192,1024]{1,0:T(8,128)} async-done(((f32[192,1024]{1,0:T(8,128)}), f32[192,1024]{1,0:T(8,128)}) %all-reduce.7.cloned.1.call-update) | async-done | bytes 786448 | tf_op jit(solution)/shard_map/psum | solution.py:31
  380.5 1.4 fusion.1
  381.9 11.7 %all-reduce = (f32[192,1]{0,1:T(1,128)S(1)}, f32[192,1]{0,1:T(1,128)S(1)}) all-reduce(f32[192,1]{0,1:T(1,128)S(1)} %bitcast.23, f32[192,1]{0,1:T(1,128)S(1)} %bitcast.22), channel_id=1, replica_groups=mesh['ra'=4,'cb'=4,'dp'=2] {'ra'}, use_global_device_ids=true, to_apply=%region_13.14 | all-reduce | flops 384 | bytes 3072 | tf_op jit(solution)/shard_map/psum | solution.py:10
  393.7 2.1 add_convert_fusion
  (26 shorter events, 0.4 us)
Async XLA Ops:
  6.5 5.5 %copy-start = (bf16[192,1024]{1,0:T(8,128)(2,1)S(1)}, bf16[192,1024]{1,0:T(8,128)(2,1)}, u32[]{:S(2)}) copy-start(bf16[192,1024]{1,0:T(8,128)(2,1)} %param.11) | copy-start | bytes 1179652
  6.5 53.0 %reduce-scatter.5.cloned.1.call-start = ((), (), s32[]{:S(2)}) async-start(), calls=%async_computation.4 | async-start | bytes 2703360 | tf_op jit(solution)/shard_map/reduce_scatter | solution.py:24
  12.0 93.8 %reduce-scatter.7.cloned.1.call-start = ((), (), s32[]{:S(2)}) async-start(), calls=%async_computation.5 | async-start | bytes 2703360 | tf_op jit(solution)/shard_map/reduce_scatter | solution.py:25
  17.4 118.4 %all-gather.3.cloned.1.call-start = ((), (), s32[]{:S(2)}) async-start(), calls=%async_computation.6 | async-start | bytes 1351680 | tf_op jit(solution)/shard_map/all_gather | solution.py:29
  107.9 94.5 %copy-start.1 = (f32[1024]{0:T(1024)S(1)}, f32[1024]{0:T(1024)}, u32[]{:S(2)}) copy-start(f32[1024]{0:T(1024)} %param.16) | copy-start | bytes 12292
  107.9 94.5 %copy-start.2 = (f32[1024]{0:T(1024)S(1)}, f32[1024]{0:T(1024)}, u32[]{:S(2)}) copy-start(f32[1024]{0:T(1024)} %param.15) | copy-start | bytes 12292
  107.9 81.3 %all-reduce.5.cloned.1.call-start = ((), (), s32[]{:S(2)}) async-start(), calls=%async_computation.7 | async-start | bytes 1572864 | tf_op jit(solution)/shard_map/psum | solution.py:31
  141.0 110.0 %reduce-scatter.11.cloned.1.call-start = ((), (), s32[]{:S(2)}) async-start(), calls=%async_computation.9 | async-start | bytes 2703360 | tf_op jit(solution)/shard_map/reduce_scatter | solution.py:25
  209.0 88.1 %reduce-scatter.9.cloned.1.call-start = ((), (), s32[]{:S(2)}) async-start(), calls=%async_computation.8 | async-start | bytes 2703360 | tf_op jit(solution)/shard_map/reduce_scatter | solution.py:24
  214.4 112.8 %all-gather.5.cloned.1.call-start = ((), (), s32[]{:S(2)}) async-start(), calls=%async_computation.10 | async-start | bytes 1351680 | tf_op jit(solution)/shard_map/all_gather | solution.py:29
  299.2 94.5 %copy-start.3 = (f32[1024]{0:T(1024)S(1)}, f32[1024]{0:T(1024)}, u32[]{:S(2)}) copy-start(f32[1024]{0:T(1024)} %param.21) | copy-start | bytes 12292
  299.2 94.4 %copy-start.4 = (f32[1024]{0:T(1024)S(1)}, f32[1024]{0:T(1024)}, u32[]{:S(2)}) copy-start(f32[1024]{0:T(1024)} %param.20) | copy-start | bytes 12292
  299.3 81.3 %all-reduce.7.cloned.1.call-start = ((), (), s32[]{:S(2)}) async-start(), calls=%async_computation.11 | async-start | bytes 1572864 | tf_op jit(solution)/shard_map/psum | solution.py:31
Sparse Core Ops, SparseCore 0:
  12.1 47.3 reduce-scatter.4
  61.8 43.8 reduce-scatter.6
  108.0 27.7 all-gather.2
  141.1 47.9 all-reduce.4
  209.1 41.8 reduce-scatter.10
  253.2 43.8 reduce-scatter.8
  299.4 27.7 all-gather.4
  332.5 47.9 all-reduce.6
where the time goes:
time: 403 us
  waiting for transfers between devices  323 us (80%)
  matrix products  31.6 us (8%)
  blocking collectives  23.5 us (6%)
  between operations  13.6 us (3%)
  other arithmetic  10.5 us (3%)
    psum x2, waiting for transfers between devices, half_step(): branch = lax.psum(partial_value, 'cb')  96.3 us
    reduce_scatter x2, waiting for transfers between devices, half_step(): lax.psum_scatter(gate_part, 'ra', scatter_dimension=0, tiled=True)  88.2 us
    reduce_scatter x2, waiting for transfers between devices, half_step(): lax.psum_scatter(up_part, 'ra', scatter_dimension=0, tiled=True)  82.9 us
    all_gather x2, waiting for transfers between devices, half_step(): lax.all_gather(hidden, 'ra', axis=0, tiled=True)  55.7 us
    psum x2, blocking collectives, normalize(): lax.psum((jnp.sum(mixed, axis=-1, keepdims=True), jnp.sum(mixed * mixed,...  23.5 us
    dot_general x2, matrix products, half_step(): gate_part = jnp.dot(values, gate, preferred_element_type=jnp.float32)  10.7 us
    dot_general x2, matrix products, half_step(): up_part = jnp.dot(values, up, preferred_element_type=jnp.float32)  10.5 us
    dot_general x2, matrix products, half_step(): jnp.dot(lax.all_gather(hidden, 'ra', axis=0, tiled=True), down, preferred...  10.4 us
  transfers between devices with their start and end apart: 8, of which 8 were waited for; matrix products, arithmetic and copies ran while one was open for 3% of the time, Pallas kernels for 0%

commit v1 on v0

v1 whole, which is shorter than its diff:
```python
import functools

import jax
import jax.numpy as jnp
from jax import lax
from jax.experimental import pallas as pl
from jax.experimental.pallas import tpu as pltpu
from jax.sharding import PartitionSpec as P

F32 = jnp.float32
BF16 = jnp.bfloat16
SKEW = 2
FLOW = (F32, BF16)
FOLD = (F32, F32)
LAYERS = 2


def dot(a, b):
    return jnp.dot(a, b, preferred_element_type=F32)


def kernel(
    R, C, D, chunks, width,
    tokens, g0, u0, d0, gain0, shift0, g1, u1, d1, gain1, shift1,
    out,
    v, wg, wu, wd, part, flow0, flow1, hid, acc, cs0, cs1, cr0, cr1, stat,
    sem_v, sem_g, sem_u, sem_d,
    flow_s, flow_r, hid_s, hid_r, fold_s, fold_r, stat_s, stat_r,
):
    r = lax.axis_index("ra")
    c = lax.axis_index("cb")
    rows = tokens.shape[0]
    half = rows // 2
    bits = C.bit_length() - 1
    gates, ups, downs = (g0, g1), (u0, u1), (d0, d1)
    gains, shifts = (gain0, gain1), (shift0, shift1)
    flows, css, crs = (flow0, flow1), (cs0, cs1), (cr0, cr1)

    def partner(k):
        m = 2**k
        return c + m - 2 * m * ((c // m) % 2)

    load_v = pltpu.make_async_copy(tokens, v, sem_v)
    load_v.start()

    def load_gate(l, j):
        return pltpu.make_async_copy(
            gates[l].at[:, pl.ds(pl.multiple_of(j * width, width), width)], wg.at[l, j], sem_g.at[l, j]
        )

    def load_up(l, j):
        return pltpu.make_async_copy(
            ups[l].at[:, pl.ds(pl.multiple_of(j * width, width), width)], wu.at[l, j], sem_u.at[l, j]
        )

    def load_down(l, j):
        return pltpu.make_async_copy(
            downs[l].at[pl.ds(pl.multiple_of(j * width, width), width)], wd.at[l, j], sem_d.at[l, j]
        )

    def begin(l):
        @pl.loop(0, chunks)
        def _(j):
            load_gate(l, j).start()
            load_up(l, j).start()

        @pl.loop(0, chunks)
        def _(j):
            load_down(l, j).start()

    begin(0)

    barrier = pltpu.get_barrier_semaphore()
    for o in range(1, R):
        pl.semaphore_signal(barrier, inc=1, device_id={"ra": (r + o) % R})
    for k in range(bits):
        pl.semaphore_signal(barrier, inc=1, device_id={"cb": partner(k)})
    pl.semaphore_wait(barrier, R - 1 + bits)

    load_v.wait()

    for l in range(LAYERS):
        flow, cs, cr = flows[l], css[l], crs[l]

        def step_of(d):
            return 1 - 2 * d

        def send_flow(d, j):
            return pltpu.make_async_remote_copy(
                src_ref=flow.at[d, j], dst_ref=flow.at[d, j],
                send_sem=flow_s.at[l, d, j], recv_sem=flow_r.at[l, d, j],
                device_id={"ra": (r + step_of(d) + R) % R},
            )

        def send_hid(d, j):
            return pltpu.make_async_remote_copy(
                src_ref=hid.at[l, d, j], dst_ref=hid.at[l, d, j],
                send_sem=hid_s.at[l, d, j], recv_sem=hid_r.at[l, d, j],
                device_id={"ra": (r - step_of(d) + R) % R},
            )

        @pl.loop(0, chunks)
        def _(j):
            load_gate(l, j).wait()
            load_up(l, j).wait()
            gate_part = dot(v[...], wg[l, j])
            up_part = dot(v[...], wu[l, j])
            for d in range(2):
                lo = (1 - d) * half
                first = r == d * (R - 1)
                a = gate_part[lo:lo + half]
                b = up_part[lo:lo + half]

                @pl.when(first)
                def _():
                    flow[d, j, :, :width] = a.astype(flow.dtype)
                    flow[d, j, :, width:] = b.astype(flow.dtype)
                    send_flow(d, j).start()

                @pl.when(jnp.logical_not(first))
                def _():
                    part[d, j, :, :width] = a
                    part[d, j, :, width:] = b

        if l + 1 < LAYERS:
            begin(l + 1)

        acc[...] = jnp.zeros_like(acc)

        @pl.loop(0, chunks)
        def _(j):
            load_down(l, j).wait()

        @pl.loop(0, chunks + 2 * (R - 1) * SKEW)
        def _(t):
            for d in range(2):
                place = r if d == 0 else R - 1 - r
                j = t - place * SKEW

                @pl.when((place > 0) & (j >= 0) & (j < chunks))
                def _():
                    send_flow(d, j).wait_recv()
                    total = flow[d, j].astype(F32) + part[d, j]

                    @pl.when(place < R - 1)
                    def _():
                        flow[d, j] = total.astype(flow.dtype)
                        send_flow(d, j).start()

                    @pl.when(place == R - 1)
                    def _():
                        gate_pre = total[:, :width]
                        up_pre = total[:, width:]
                        hid[l, d, j] = (jax.nn.silu(gate_pre) * up_pre).astype(BF16)

            for d in range(2):
                place = r if d == 0 else R - 1 - r
                back = R - 1 - place
                i = t - (R - 1) * SKEW - back * SKEW

                @pl.when((i >= 0) & (i < chunks))
                def _():
                    @pl.when(back > 0)
                    def _():
                        send_hid(d, i).wait_recv()

                    @pl.when(place > 0)
                    def _():
                        send_hid(d, i).start()

                    acc[d] += dot(hid[l, d, i], wd[l, i])

        def send_fold(d, k):
            return pltpu.make_async_remote_copy(
                src_ref=cs.at[d, k], dst_ref=cr.at[d, k],
                send_sem=fold_s.at[l, d, k], recv_sem=fold_r.at[l, d, k],
                device_id={"cb": partner((k + d) % bits)},
            )

        for d in range(2):
            cs[d, 0] = acc[d].astype(cs.dtype)
            send_fold(d, 0).start()
        for k in range(bits):
            for d in range(2):
                send_fold(d, k).wait_recv()
                total = cs[d, k].astype(F32) + cr[d, k].astype(F32)
                if k + 1 < bits:
                    cs[d, k + 1] = total.astype(cs.dtype)
                    send_fold(d, k + 1).start()
                else:
                    lo = (1 - d) * half
                    acc[d] = 0.25 * v[lo:lo + half].astype(F32) + 0.5 * total

        padded = stat.shape[-1]
        sums = []
        for d in (1, 0):
            m = acc[d]
            sums.append((jnp.sum(m, axis=-1, keepdims=True), jnp.sum(m * m, axis=-1, keepdims=True)))
        ones = jnp.concatenate([s[0] for s in sums] + ([jnp.zeros((padded - rows, 1), F32)] if padded > rows else []))
        twos = jnp.concatenate([s[1] for s in sums] + ([jnp.zeros((padded - rows, 1), F32)] if padded > rows else []))
        lane = lax.broadcasted_iota(jnp.int32, (padded, 128), 1)
        mine = jnp.where(lane == 0, ones, twos).T[:8]
        stat[l, r] = mine

        def send_stat(o):
            return pltpu.make_async_remote_copy(
                src_ref=stat.at[l, r], dst_ref=stat.at[l, r],
                send_sem=stat_s.at[l, o], recv_sem=stat_r.at[l, r],
                device_id={"ra": (r + o) % R},
            )

        def recv_stat(o):
            src = (r + o) % R
            return pltpu.make_async_remote_copy(
                src_ref=stat.at[l, src], dst_ref=stat.at[l, src],
                send_sem=stat_s.at[l, o], recv_sem=stat_r.at[l, src],
                device_id={"ra": src},
            )

        for o in range(1, R):
            send_stat(o).start()
        @pl.loop(0, chunks)
        def _(j):
            for d in range(2):
                place = r if d == 0 else R - 1 - r

                @pl.when(place < R - 1)
                def _():
                    send_flow(d, j).wait_send()

                @pl.when(place > 0)
                def _():
                    send_hid(d, j).wait_send()

        for d in range(2):
            for k in range(bits):
                send_fold(d, k).wait_send()
        for o in range(1, R):
            recv_stat(o).wait_recv()
        whole = stat[l, 0]
        for q in range(1, R):
            whole = whole + stat[l, q]
        mean = whole / D
        row = lax.broadcasted_iota(jnp.int32, whole.shape, 0)
        variance = mean - jnp.where(row == 1, 1.0, 0.0) * (mean[:1] * mean[:1])
        both = jnp.where(row == 1, lax.rsqrt(variance + 1e-05), mean)
        cols = jnp.concatenate([both] * 16, axis=0).T
        target = v if l + 1 < LAYERS else out
        for d in range(2):
            lo = (1 - d) * half
            centre = cols[lo:lo + half, 0:1]
            scale = cols[lo:lo + half, 1:2]
            normed = (acc[d] - centre) * scale * gains[l][...] + shifts[l][...]
            target[lo:lo + half] = normed.astype(BF16)
        for o in range(1, R):
            send_stat(o).wait_send()


def on_device(R, C, D, *args):
    tokens, g0, u0, d0, a0, b0, g1, u1, d1, a1, b1 = args
    rows, depth = tokens.shape
    ff = g0.shape[1]
    width = 256 if ff % 256 == 0 else 128
    chunks = ff // width
    half = rows // 2
    bits = C.bit_length() - 1
    padded = -(-rows // 128) * 128
    vmem = pl.BlockSpec(memory_space=pltpu.VMEM)
    hbm = pl.BlockSpec(memory_space=pl.ANY)
    L = LAYERS
    dma = pltpu.SemaphoreType.DMA
    line = lambda x: x.reshape(1, depth)
    return pl.pallas_call(
        functools.partial(kernel, R, C, D, chunks, width),
        out_shape=jax.ShapeDtypeStruct((rows, depth), BF16),
        in_specs=[hbm, hbm, hbm, hbm, vmem, vmem, hbm, hbm, hbm, vmem, vmem],
        out_specs=vmem,
        scratch_shapes=[
            pltpu.VMEM((rows, depth), BF16),
            pltpu.VMEM((L, chunks, depth, width), BF16),
            pltpu.VMEM((L, chunks, depth, width), BF16),
            pltpu.VMEM((L, chunks, width, depth), BF16),
            pltpu.VMEM((2, chunks, half, 2 * width), F32),
            pltpu.VMEM((2, chunks, half, 2 * width), FLOW[0]),
            pltpu.VMEM((2, chunks, half, 2 * width), FLOW[1]),
            pltpu.VMEM((L, 2, chunks, half, width), BF16),
            pltpu.VMEM((2, half, depth), F32),
            pltpu.VMEM((2, bits, half, depth), FOLD[0]),
            pltpu.VMEM((2, bits, half, depth), FOLD[1]),
            pltpu.VMEM((2, bits, half, depth), FOLD[0]),
            pltpu.VMEM((2, bits, half, depth), FOLD[1]),
            pltpu.VMEM((L, R, 8, padded), F32),
            dma,
            dma((L, chunks)),
            dma((L, chunks)),
            dma((L, chunks)),
            dma((L, 2, chunks)),
            dma((L, 2, chunks)),
            dma((L, 2, chunks)),
            dma((L, 2, chunks)),
            dma((L, 2, bits)),
            dma((L, 2, bits)),
            dma((L, R)),
            dma((L, R)),
        ],
        compiler_params=pltpu.CompilerParams(
            collective_id=0, has_side_effects=True, vmem_limit_bytes=67043328
        ),
    )(tokens, g0, u0, d0, line(a0), line(b0), g1, u1, d1, line(a1), line(b1))


def solution(mesh):
    in_specs = (
        P("dp", "ra"),
        P("ra", "cb"),
        P("ra", "cb"),
        P("cb", "ra"),
        P("ra"),
        P("ra"),
        P("ra", "cb"),
        P("ra", "cb"),
        P("cb", "ra"),
        P("ra"),
        P("ra"),
    )

    def step(tokens, *rest):
        R, C = mesh.shape["ra"], mesh.shape["cb"]
        return on_device(R, C, tokens.shape[1] * R, tokens, *rest)

    return jax.shard_map(
        step, mesh=mesh, in_specs=in_specs, out_specs=P("dp", "ra"), check_vma=False
    )
```

time: 403 us -> 191 us (0.47)
  waiting for transfers between devices: 323 us -> 0 us
  Pallas kernels: 0 us -> 190 us
  matrix products: 31.6 us -> 0 us
  blocking collectives: 23.5 us -> 0 us
  between operations: 13.6 us -> 0.01 us
  other arithmetic: 10.5 us -> 0 us
    pallas_call x0 -> x1, Pallas kernels: none -> 190 us  [on_device(): pl.pallas_call(functools.partial(kernel, R, C, D, chunks, width), out_sha...]
    reduce_scatter x4 -> x0, waiting for transfers between devices: 171 us -> none  [the longest x2 88.2 us: half_step(): lax.psum_scatter(gate_part, 'ra', scatter_dimension=0, tiled=True)]
    psum x2 -> x0, waiting for transfers between devices: 96.3 us -> none  [half_step(): branch = lax.psum(partial_value, 'cb')]
    all_gather x2 -> x0, waiting for transfers between devices: 55.7 us -> none  [half_step(): lax.all_gather(hidden, 'ra', axis=0, tiled=True)]
    dot_general x6 -> x0, matrix products: 31.6 us -> none  [the longest x2 10.7 us: half_step(): gate_part = jnp.dot(values, gate, preferred_element_type=jnp.float32)]
    psum x2 -> x0, blocking collectives: 23.5 us -> none  [normalize(): lax.psum((jnp.sum(mixed, axis=-1, keepdims=True), jnp.sum(mixed * mixed,...]
    convert_element_type x4 -> x0, other arithmetic: 7.63 us -> none  [the longest x2 4.14 us: half_step(): hidden = (jax.nn.silu(gate_pre) * up_pre).astype(jnp.bfloat16)]
  transfers between devices with their start and end apart: 8 -> 0, of which waited for: 8 -> 0; matrix products, arithmetic and copies ran while one was open for 3% -> 0% of each run, Pallas kernels for 0% -> 0%
where the time goes in v1:
time: 191 us
  Pallas kernels  190 us (99%)
    pallas_call x1, Pallas kernels, on_device(): pl.pallas_call(functools.partial(kernel, R, C, D, chunks, width), out_sha...  190 us

profile of v1, /device:TPU:0, one launch (start us, length us, event | category | flops | bytes accessed | tf_op | source)
XLA Modules:
  0.0 191.3 jit_solution(10417633557217542725)
XLA Ops:
  0.0 189.5 %shard_map.109 = bf16[192,1024]{1,0:T(8,128)(2,1)} custom-call(bf16[192,1024]{1,0:T(8,128)(2,1)} %tokens.1, bf16[1024,2816]{1,0:T(8,128)(2,1)} %g0.1, bf16[1024,2816]{1,0:T(8,128)(2,1)} %u0.1, bf16[2816,1024]{1,0:T(8,128)(2,1)} %d0.1, f32[1,1024]{1,0:T(1,128)} %bitcast.4, f32[1,1024]{1,0:T(1,128)} %bitcast.5, bf16[1024,2816]{1,0:T(8,128)(2,1)} %g1.1, ...), custom_call_target="tpu_custom_call" | custom-call | tf_op jit(solution)/shard_map/pallas_call | solution.py:273
  189.5 1.8 copy.13

commit v2 on v0

v2 whole, which is shorter than its diff:
```python
import functools

import jax
import jax.numpy as jnp
from jax import lax
from jax.experimental import pallas as pl
from jax.experimental.pallas import tpu as pltpu
from jax.sharding import PartitionSpec as P

F32 = jnp.float32
BF16 = jnp.bfloat16
SKEW = 3
NARROW = (4, 11)
FOLD = (F32, BF16)
LAYERS = 2
GROUPS = 1


def dot(a, b):
    return jnp.dot(a, b, preferred_element_type=F32)


def kernel(
    R, C, D, chunks, width,
    tokens, g0, u0, d0, gain0, shift0, g1, u1, d1, gain1, shift1,
    out,
    v, wg, wu, wd, part, flow0, flow0n, flow1, hid, acc, cs0, cs1, cr0, cr1, stat,
    sem_v, sem_g, sem_u, sem_d,
    flow_s, flow_r, hid_s, hid_r, fold_s, fold_r, stat_s, stat_r,
):
    r = lax.axis_index("ra")
    c = lax.axis_index("cb")
    rows = tokens.shape[0]
    span = rows // GROUPS
    half = span // 2
    total_chunks = GROUPS * chunks
    bits = C.bit_length() - 1
    gates, ups, downs = (g0, g1), (u0, u1), (d0, d1)
    gains, shifts = (gain0, gain1), (shift0, shift1)
    css, crs = (cs0, cs1), (cr0, cr1)
    narrow = flow0n.shape[1]
    flows = (
        ((flow0n, 0, narrow), (flow0, narrow, total_chunks)),
        ((flow1, 0, total_chunks),),
    )

    def partner(k):
        m = 2**k
        return c + m - 2 * m * ((c // m) % 2)

    load_v = pltpu.make_async_copy(tokens, v, sem_v)
    load_v.start()

    def load_gate(l, j):
        return pltpu.make_async_copy(
            gates[l].at[:, pl.ds(pl.multiple_of(j * width, width), width)], wg.at[l, j], sem_g.at[l, j]
        )

    def load_up(l, j):
        return pltpu.make_async_copy(
            ups[l].at[:, pl.ds(pl.multiple_of(j * width, width), width)], wu.at[l, j], sem_u.at[l, j]
        )

    def load_down(l, j):
        return pltpu.make_async_copy(
            downs[l].at[pl.ds(pl.multiple_of(j * width, width), width)], wd.at[l, j], sem_d.at[l, j]
        )

    def begin(l):
        @pl.loop(0, chunks)
        def _(j):
            load_gate(l, j).start()
            load_up(l, j).start()

        @pl.loop(0, chunks)
        def _(j):
            load_down(l, j).start()

    begin(0)

    barrier = pltpu.get_barrier_semaphore()
    for o in range(1, R):
        pl.semaphore_signal(barrier, inc=1, device_id={"ra": (r + o) % R})
    for k in range(bits):
        pl.semaphore_signal(barrier, inc=1, device_id={"cb": partner(k)})
    pl.semaphore_wait(barrier, R - 1 + bits)

    load_v.wait()

    def step_of(d):
        return 1 - 2 * d

    def send_flow(l, d, q, ref, lo):
        return pltpu.make_async_remote_copy(
            src_ref=ref.at[d, q - lo], dst_ref=ref.at[d, q - lo],
            send_sem=flow_s.at[l, d, q], recv_sem=flow_r.at[l, d, q],
            device_id={"ra": (r + step_of(d) + R) % R},
        )

    def send_hid(l, d, q):
        return pltpu.make_async_remote_copy(
            src_ref=hid.at[l, d, q], dst_ref=hid.at[l, d, q],
            send_sem=hid_s.at[l, d, q], recv_sem=hid_r.at[l, d, q],
            device_id={"ra": (r - step_of(d) + R) % R},
        )

    def expand(l, first_group, groups, fresh):
        top = first_group * span

        @pl.loop(0, chunks)
        def _(j):
            if fresh:
                load_gate(l, j).wait()
                load_up(l, j).wait()
            x = v[top:top + groups * span]
            gate_part = dot(x, wg[l, j])
            up_part = dot(x, wu[l, j])
            for g in range(groups):
                q = (first_group + g) * chunks + j
                for d in range(2):
                    lo = g * span + (1 - d) * half
                    first = r == d * (R - 1)
                    a = gate_part[lo:lo + half]
                    b = up_part[lo:lo + half]

                    for flow, begins, ends in flows[l]:
                        @pl.when(first & (q >= begins) & (q < ends))
                        def _():
                            flow[d, q - begins, :, :width] = a.astype(flow.dtype)
                            flow[d, q - begins, :, width:] = b.astype(flow.dtype)
                            send_flow(l, d, q, flow, begins).start()

                    @pl.when(jnp.logical_not(first))
                    def _():
                        part[d, q, :, :width] = a
                        part[d, q, :, width:] = b

    def send_fold(l, g, d, k):
        return pltpu.make_async_remote_copy(
            src_ref=css[l].at[g, d, k], dst_ref=crs[l].at[g, d, k],
            send_sem=fold_s.at[l, g, d, k], recv_sem=fold_r.at[l, g, d, k],
            device_id={"cb": partner((k + d) % bits)},
        )

    def fold_begin(l, g):
        for d in range(2):
            css[l][g, d, 0] = acc[g, d].astype(css[l].dtype)
            send_fold(l, g, d, 0).start()

    def fold_step(l, g, k):
        cs, cr = css[l], crs[l]
        for d in range(2):
            send_fold(l, g, d, k).wait_recv()
            total = cs[g, d, k].astype(F32) + cr[g, d, k].astype(F32)
            if k + 1 < bits:
                cs[g, d, k + 1] = total.astype(cs.dtype)
                send_fold(l, g, d, k + 1).start()
            else:
                lo = g * span + (1 - d) * half
                acc[g, d] = 0.25 * v[lo:lo + half].astype(F32) + 0.5 * total
        if k + 1 == bits:
            stat_begin(l, g)

    def send_stat(l, g, o):
        return pltpu.make_async_remote_copy(
            src_ref=stat.at[l, g, r], dst_ref=stat.at[l, g, r],
            send_sem=stat_s.at[l, g, o], recv_sem=stat_r.at[l, g, r],
            device_id={"ra": (r + o) % R},
        )

    def recv_stat(l, g, o):
        src = (r + o) % R
        return pltpu.make_async_remote_copy(
            src_ref=stat.at[l, g, src], dst_ref=stat.at[l, g, src],
            send_sem=stat_s.at[l, g, o], recv_sem=stat_r.at[l, g, src],
            device_id={"ra": src},
        )

    def stat_begin(l, g):
        padded = stat.shape[-1]
        sums = []
        for d in (1, 0):
            m = acc[g, d]
            sums.append((jnp.sum(m, axis=-1, keepdims=True), jnp.sum(m * m, axis=-1, keepdims=True)))
        rest = [jnp.zeros((padded - span, 1), F32)] if padded > span else []
        ones = jnp.concatenate([s[0] for s in sums] + rest)
        twos = jnp.concatenate([s[1] for s in sums] + rest)
        lane = lax.broadcasted_iota(jnp.int32, (padded, 128), 1)
        stat[l, g, r] = jnp.where(lane == 0, ones, twos).T[:8]
        for o in range(1, R):
            send_stat(l, g, o).start()

    def finish(l, g):
        for o in range(1, R):
            recv_stat(l, g, o).wait_recv()
        whole = stat[l, g, 0]
        for q in range(1, R):
            whole = whole + stat[l, g, q]
        mean = whole / D
        row = lax.broadcasted_iota(jnp.int32, whole.shape, 0)
        variance = mean - jnp.where(row == 1, 1.0, 0.0) * (mean[:1] * mean[:1])
        both = jnp.where(row == 1, lax.rsqrt(variance + 1e-05), mean)
        cols = jnp.concatenate([both] * 16, axis=0).T
        target = v if l + 1 < LAYERS else out
        for d in range(2):
            lo = (1 - d) * half
            centre = cols[lo:lo + half, 0:1]
            scale = cols[lo:lo + half, 1:2]
            normed = (acc[g, d] - centre) * scale * gains[l][...] + shifts[l][...]
            target[g * span + lo:g * span + lo + half] = normed.astype(BF16)

    expand(0, 0, GROUPS, True)
    last = GROUPS - 1
    lag = chunks + 2 * (R - 1) * SKEW
    gap = max(1, chunks // (bits + 1))
    steps = max(total_chunks + 2 * (R - 1) * SKEW, lag + last * chunks - chunks + gap * (bits + 1) + 1)
    for l in range(LAYERS):
        if l + 1 < LAYERS:
            begin(l + 1)

        acc[...] = jnp.zeros_like(acc)

        @pl.loop(0, chunks)
        def _(j):
            load_down(l, j).wait()

        @pl.loop(0, steps)
        def _(t):
            for d in range(2):
                place = r if d == 0 else R - 1 - r
                j = t - place * SKEW

                for flow, begins, ends in flows[l]:
                    @pl.when((place > 0) & (j >= begins) & (j < ends))
                    def _():
                        send_flow(l, d, j, flow, begins).wait_recv()
                        total = flow[d, j - begins].astype(F32) + part[d, j]

                        @pl.when(place < R - 1)
                        def _():
                            flow[d, j - begins] = total.astype(flow.dtype)
                            send_flow(l, d, j, flow, begins).start()

                        @pl.when(place == R - 1)
                        def _():
                            gate_pre = total[:, :width]
                            up_pre = total[:, width:]
                            hid[l, d, j] = (jax.nn.silu(gate_pre) * up_pre).astype(BF16)

            for d in range(2):
                place = r if d == 0 else R - 1 - r
                back = R - 1 - place
                i = t - (R - 1) * SKEW - back * SKEW

                @pl.when((i >= 0) & (i < total_chunks))
                def _():
                    @pl.when(back > 0)
                    def _():
                        send_hid(l, d, i).wait_recv()

                    @pl.when(place > 0)
                    def _():
                        send_hid(l, d, i).start()

                    g = i // chunks
                    acc[g, d] += dot(hid[l, d, i], wd[l, i - g * chunks])

            for g in range(last):
                at = lag + g * chunks

                @pl.when(t == at)
                def _():
                    fold_begin(l, g)

                for k in range(bits):
                    @pl.when(t == at + gap * (k + 1))
                    def _():
                        fold_step(l, g, k)

                @pl.when(t == at + gap * (bits + 1))
                def _():
                    finish(l, g)

        fold_begin(l, last)
        if l + 1 < LAYERS and last > 0:
            expand(l + 1, 0, last, True)
        for k in range(bits):
            fold_step(l, last, k)

        @pl.loop(0, total_chunks)
        def _(j):
            for d in range(2):
                place = r if d == 0 else R - 1 - r

                for flow, begins, ends in flows[l]:
                    @pl.when((place < R - 1) & (j >= begins) & (j < ends))
                    def _():
                        send_flow(l, d, j, flow, begins).wait_send()

                @pl.when(place > 0)
                def _():
                    send_hid(l, d, j).wait_send()

        finish(l, last)
        if l + 1 < LAYERS:
            expand(l + 1, last, 1, last == 0)
        for g in range(GROUPS):
            for d in range(2):
                for k in range(bits):
                    send_fold(l, g, d, k).wait_send()
            for o in range(1, R):
                send_stat(l, g, o).wait_send()


def on_device(R, C, D, *args):
    tokens, g0, u0, d0, a0, b0, g1, u1, d1, a1, b1 = args
    rows, depth = tokens.shape
    ff = g0.shape[1]
    width = 256 if ff % 256 == 0 else 128
    chunks = ff // width
    span = rows // GROUPS
    half = span // 2
    bits = C.bit_length() - 1
    padded = -(-span // 128) * 128
    Q = GROUPS * chunks
    narrow = Q * NARROW[0] // NARROW[1]
    vmem = pl.BlockSpec(memory_space=pltpu.VMEM)
    hbm = pl.BlockSpec(memory_space=pl.ANY)
    L = LAYERS
    dma = pltpu.SemaphoreType.DMA
    line = lambda x: x.reshape(1, depth)
    return pl.pallas_call(
        functools.partial(kernel, R, C, D, chunks, width),
        out_shape=jax.ShapeDtypeStruct((rows, depth), BF16),
        in_specs=[hbm, hbm, hbm, hbm, vmem, vmem, hbm, hbm, hbm, vmem, vmem],
        out_specs=vmem,
        scratch_shapes=[
            pltpu.VMEM((rows, depth), BF16),
            pltpu.VMEM((L, chunks, depth, width), BF16),
            pltpu.VMEM((L, chunks, depth, width), BF16),
            pltpu.VMEM((L, chunks, width, depth), BF16),
            pltpu.VMEM((2, Q, half, 2 * width), F32),
            pltpu.VMEM((2, Q - narrow, half, 2 * width), F32),
            pltpu.VMEM((2, narrow, half, 2 * width), BF16),
            pltpu.VMEM((2, Q, half, 2 * width), BF16),
            pltpu.VMEM((L, 2, Q, half, width), BF16),
            pltpu.VMEM((GROUPS, 2, half, depth), F32),
            pltpu.VMEM((GROUPS, 2, bits, half, depth), FOLD[0]),
            pltpu.VMEM((GROUPS, 2, bits, half, depth), FOLD[1]),
            pltpu.VMEM((GROUPS, 2, bits, half, depth), FOLD[0]),
            pltpu.VMEM((GROUPS, 2, bits, half, depth), FOLD[1]),
            pltpu.VMEM((L, GROUPS, R, 8, padded), F32),
            dma,
            dma((L, chunks)),
            dma((L, chunks)),
            dma((L, chunks)),
            dma((L, 2, Q)),
            dma((L, 2, Q)),
            dma((L, 2, Q)),
            dma((L, 2, Q)),
            dma((L, GROUPS, 2, bits)),
            dma((L, GROUPS, 2, bits)),
            dma((L, GROUPS, R)),
            dma((L, GROUPS, R)),
        ],
        compiler_params=pltpu.CompilerParams(
            collective_id=0, has_side_effects=True, vmem_limit_bytes=67043328
        ),
    )(tokens, g0, u0, d0, line(a0), line(b0), g1, u1, d1, line(a1), line(b1))


def solution(mesh):
    in_specs = (
        P("dp", "ra"),
        P("ra", "cb"),
        P("ra", "cb"),
        P("cb", "ra"),
        P("ra"),
        P("ra"),
        P("ra", "cb"),
        P("ra", "cb"),
        P("cb", "ra"),
        P("ra"),
        P("ra"),
    )

    def step(tokens, *rest):
        R, C = mesh.shape["ra"], mesh.shape["cb"]
        return on_device(R, C, tokens.shape[1] * R, tokens, *rest)

    return jax.shard_map(
        step, mesh=mesh, in_specs=in_specs, out_specs=P("dp", "ra"), check_vma=False
    )
```

time: 403 us -> 166 us (0.41)
  waiting for transfers between devices: 323 us -> 0 us
  Pallas kernels: 0 us -> 164 us
  matrix products: 31.6 us -> 0 us
  blocking collectives: 23.5 us -> 0 us
  between operations: 13.6 us -> 0.01 us
  other arithmetic: 10.5 us -> 0 us
    reduce_scatter x4 -> x0, waiting for transfers between devices: 171 us -> none  [the longest x2 88.2 us: half_step(): lax.psum_scatter(gate_part, 'ra', scatter_dimension=0, tiled=True)]
    pallas_call x0 -> x1, Pallas kernels: none -> 164 us  [on_device(): pl.pallas_call(functools.partial(kernel, R, C, D, chunks, width), out_sha...]
    psum x2 -> x0, waiting for transfers between devices: 96.3 us -> none  [half_step(): branch = lax.psum(partial_value, 'cb')]
    all_gather x2 -> x0, waiting for transfers between devices: 55.7 us -> none  [half_step(): lax.all_gather(hidden, 'ra', axis=0, tiled=True)]
    dot_general x6 -> x0, matrix products: 31.6 us -> none  [the longest x2 10.7 us: half_step(): gate_part = jnp.dot(values, gate, preferred_element_type=jnp.float32)]
    psum x2 -> x0, blocking collectives: 23.5 us -> none  [normalize(): lax.psum((jnp.sum(mixed, axis=-1, keepdims=True), jnp.sum(mixed * mixed,...]
    convert_element_type x4 -> x0, other arithmetic: 7.63 us -> none  [the longest x2 4.14 us: half_step(): hidden = (jax.nn.silu(gate_pre) * up_pre).astype(jnp.bfloat16)]
  transfers between devices with their start and end apart: 8 -> 0, of which waited for: 8 -> 0; matrix products, arithmetic and copies ran while one was open for 3% -> 0% of each run, Pallas kernels for 0% -> 0%
where the time goes in v2:
time: 166 us
  Pallas kernels  164 us (99%)
  local copies, waits for them, and re-layouts  1.77 us (1%)
    pallas_call x1, Pallas kernels, on_device(): pl.pallas_call(functools.partial(kernel, R, C, D, chunks, width), out_sha...  164 us

profile of v2, /device:TPU:0, one launch (start us, length us, event | category | flops | bytes accessed | tf_op | source)
XLA Modules:
  0.0 166.1 jit_solution(14327512362880086173)
XLA Ops:
  0.0 164.3 %shard_map.109 = bf16[192,1024]{1,0:T(8,128)(2,1)} custom-call(bf16[192,1024]{1,0:T(8,128)(2,1)} %tokens.1, bf16[1024,2816]{1,0:T(8,128)(2,1)} %g0.1, bf16[1024,2816]{1,0:T(8,128)(2,1)} %u0.1, bf16[2816,1024]{1,0:T(8,128)(2,1)} %d0.1, f32[1,1024]{1,0:T(1,128)} %bitcast.4, f32[1,1024]{1,0:T(1,128)} %bitcast.5, bf16[1024,2816]{1,0:T(8,128)(2,1)} %g1.1, ...), custom_call_target="tpu_custom_call" | custom-call | tf_op jit(solution)/shard_map/pallas_call | solution.py:332
  164.3 1.8 %copy.13 = bf16[192,1024]{1,0:T(8,128)(2,1)} copy(bf16[192,1024]{1,0:T(8,128)(2,1)} %shard_map.109) | data formatting | bytes 786432
